TPU v7x, 32 devices: a whole 2x2x4 slice. The times are simulated.
32 devices in a mesh: grp: 2 (over x), sp: 4 (over y, core), tp: 4 (over z).
Axes of the slice: x: 2, y: 2, z: 4, core: 2. Of those that a mesh axis runs over, the one named last changes fastest.
Arguments:
- tokens_in: bfloat16 [2048, 2048], P(('grp', 'sp'), 'tp'), parts along dimension 0, may hold values from -8 to 8
- out_gate: bfloat16 [3, 2048, 2048], P(None, 'sp', 'tp'), may hold values from -0.125 to 0.125
- in_gate: bfloat16 [3, 2048, 2048], P(None, 'sp', 'tp'), may hold values from -0.125 to 0.125
- value_proj: bfloat16 [3, 2048, 2048], P(None, 'sp', 'tp'), may hold values from -0.125 to 0.125
- mix_proj: bfloat16 [3, 2048, 2048], P(None, 'sp', 'tp'), may hold values from -0.125 to 0.125
- conv_taps: float32 [3, 3, 2048], P(None, None, 'tp'), may hold values from -3.5 to 3.5
- norm_gains: float32 [3, 2048], P(None, 'tp'), may hold values from 0.1 to 1.9
- final_gain: float32 [2048], P('tp'), may hold values from 0.1 to 1.9
Outputs:
- normed_out: bfloat16 [2048, 2048], P(('grp', 'sp'), 'tp'), parts along dimension 0
There are 2 independent parts, one for each index of `grp`. A program takes and returns all parts, laid end to end along the dimension named above; an argument that names none is the same for every part. Nothing has to cross between parts.
All inputs are finite; a program needn't handle non-finite values.
Results may differ from a plain program's by a relative error of at most 0.025.
Values may be sent and summed in bfloat16 or wider, within the bound.
A program may use at most 64 MiB of HBM per device.

v0:
```python
import jax
import jax.numpy as jnp
from jax import lax
from jax.sharding import PartitionSpec as P

D = 2048
TAPS = 3
LAYERS = 3
epsilon = 1e-06


def passed_along(shard, axis, by):
    peers = lax.axis_size(axis)
    pairs = [(i, i + by) for i in range(peers) if 0 <= i + by < peers]
    return lax.ppermute(shard, axis, pairs)


def row_scale(stream):
    squares = lax.psum(jnp.sum(stream * stream, axis=1, keepdims=True), "tp")
    return lax.rsqrt(squares / D + epsilon)


def shards(tokens_in, out_gate, in_gate, value_proj, mix_proj, conv_taps, norm_gains, final_gain):
    stream = tokens_in.astype(jnp.float32)
    row_count = stream.shape[0]
    reach = TAPS - 1
    whole = (
        lax.all_gather(out_gate, "sp", axis=1, tiled=True),
        lax.all_gather(in_gate, "sp", axis=1, tiled=True),
        lax.all_gather(value_proj, "sp", axis=1, tiled=True),
        lax.all_gather(mix_proj, "sp", axis=1, tiled=True),
    )
    for layer_index in range(LAYERS):
        scale = row_scale(stream)
        normed = (stream * norm_gains[layer_index]).astype(jnp.bfloat16)
        gathered = lax.all_gather(normed, "tp", axis=1, tiled=True)
        products = tuple(
            (
                jnp.dot(gathered, weight[layer_index], preferred_element_type=jnp.float32)
                for weight in whole[:3]
            )
        )
        out_gates, in_gates, values = [
            (product * scale).astype(jnp.bfloat16) for product in products
        ]
        product_v = (in_gates.astype(jnp.float32) * values.astype(jnp.float32)).astype(jnp.bfloat16)
        earlier = passed_along(product_v[row_count - reach :], "sp", 1)
        padded = jnp.concatenate([earlier, product_v], axis=0)
        convolved = padded[0:row_count].astype(jnp.float32) * conv_taps[layer_index, 0]
        for tap_index in range(1, TAPS):
            convolved = (
                convolved
                + padded[tap_index : tap_index + row_count].astype(jnp.float32)
                * conv_taps[layer_index, tap_index]
            )
        gated = (out_gates.astype(jnp.float32) * convolved).astype(jnp.bfloat16)
        spread = lax.all_gather(gated, "tp", axis=1, tiled=True)
        mixed = jnp.dot(spread, whole[3][layer_index], preferred_element_type=jnp.float32)
        stream = stream + mixed
    scale = row_scale(stream)
    return (stream * scale * final_gain).astype(jnp.bfloat16)


def solution(mesh):
    in_specs = (
        P(("grp", "sp"), "tp"),
        P(None, "sp", "tp"),
        P(None, "sp", "tp"),
        P(None, "sp", "tp"),
        P(None, "sp", "tp"),
        P(None, None, "tp"),
        P(None, "tp"),
        P("tp"),
    )
    out_specs = P(("grp", "sp"), "tp")
    return jax.shard_map(shards, mesh=mesh, in_specs=in_specs, out_specs=out_specs, check_vma=False)
```

profile of v0, /device:TPU:0, one launch (start us, length us, event | category | flops | bytes accessed | tf_op | source)
XLA Modules:
  0.0 424.5 jit_solution(9574232206159354128)
XLA Ops:
  6.5 0.0 all-gather.11.cloned.1.call-start
  6.5 0.8 fusion.60
  7.4 1.7 fusion.55
  9.1 0.0 all-gather.11.cloned.1.call-update
  9.1 0.0 all-gather.17.cloned.1.call-start
  9.2 0.7 all-gather.17.cloned.1.call-update
  9.9 0.0 all-gather.15.cloned.1.call-start
  9.9 0.7 all-gather.15.cloned.1.call-update
  10.6 0.0 copy-start.1
  10.6 0.0 all-gather.13.cloned.1.call-start
  10.7 0.5 all-gather.13.cloned.1.call-update
  11.2 0.0 all-gather.21.cloned.1.call-start
  11.2 0.5 all-gather.21.cloned.1.call-update
  11.8 0.0 all-gather.19.cloned.1.call-start
  11.8 13.5 %psum.28 = f32[256,1]{0,1:T(1,128)S(1)} all-reduce(f32[256,1]{0,1:T(1,128)S(1)} %bitcast.159), channel_id=1, replica_groups=mesh['grp'=2,'sp'=4,'tp'=4] {'tp'}, use_global_device_ids=true, to_apply=%region_1.0 | all-reduce | flops 256 | bytes 2048 | tf_op jit(solution)/shard_map/psum | solution.py:19
  25.3 14.7 %all-gather.11.cloned.1.call-done = bf16[256,2048]{1,0:T(8,128)(2,1)} async-done(((bf16[256,512]{1,0:T(8,128)(2,1)}), bf16[256,2048]{1,0:T(8,128)(2,1)}) %all-gather.11.cloned.1.call-update) | async-done | bytes 1048592 | tf_op jit(solution)/shard_map/all_gather | solution.py:36
  40.0 47.3 %all-gather.17.cloned.1.call-done = bf16[3,2048,512]{2,1,0:T(8,128)(2,1)} async-done(((bf16[3,512,512]{2,1,0:T(8,128)(2,1)}), bf16[3,2048,512]{2,1,0:T(8,128)(2,1)}) %all-gather.17.cloned.1.call-update) | async-done | bytes 6291472 | tf_op jit(solution)/shard_map/all_gather | solution.py:30
  87.3 2.6 fusion.39
  90.0 0.0 copy-start
  90.0 45.3 %all-gather.15.cloned.1.call-done = bf16[3,2048,512]{2,1,0:T(8,128)(2,1)} async-done(((bf16[3,512,512]{2,1,0:T(8,128)(2,1)}), bf16[3,2048,512]{2,1,0:T(8,128)(2,1)}) %all-gather.15.cloned.1.call-update) | async-done | bytes 6291472 | tf_op jit(solution)/shard_map/all_gather | solution.py:29
  135.3 2.6 fusion.38
  137.9 2.2 collective-permute-start
  140.1 0.0 copy-done.1
  140.1 43.0 %all-gather.13.cloned.1.call-done = bf16[3,2048,512]{2,1,0:T(8,128)(2,1)} async-done(((bf16[3,512,512]{2,1,0:T(8,128)(2,1)}), bf16[3,2048,512]{2,1,0:T(8,128)(2,1)}) %all-gather.13.cloned.1.call-update) | async-done | bytes 6291472 | tf_op jit(solution)/shard_map/all_gather | solution.py:28
  183.1 0.0 collective-permute-done
  183.1 0.0 copy-done.3
  183.1 3.1 fusion.35
  186.2 0.0 all-gather.19.cloned.1.call-update
  186.2 0.0 all-gather.23.cloned.1.call-start
  186.3 44.6 %all-gather.21.cloned.1.call-done = bf16[3,2048,512]{2,1,0:T(8,128)(2,1)} async-done(((bf16[3,512,512]{2,1,0:T(8,128)(2,1)}), bf16[3,2048,512]{2,1,0:T(8,128)(2,1)}) %all-gather.21.cloned.1.call-update) | async-done | bytes 6291472 | tf_op jit(solution)/shard_map/all_gather | solution.py:31
  230.9 29.4 %all-gather.19.cloned.1.call-done = bf16[256,2048]{1,0:T(8,128)(2,1)} async-done(((bf16[256,512]{1,0:T(8,128)(2,1)}), bf16[256,2048]{1,0:T(8,128)(2,1)}) %all-gather.19.cloned.1.call-update) | async-done | bytes 1048592 | tf_op jit(solution)/shard_map/all_gather | solution.py:57
  260.3 0.0 copy-done
  260.3 3.4 multiply_reduce_fusion.2
  263.7 0.0 all-gather.23.cloned.1.call-update
  263.7 0.0 all-gather.25.cloned.1.call-start
  263.8 10.3 %psum.29 = f32[256,1]{0,1:T(1,128)S(1)} all-reduce(f32[256,1]{0,1:T(1,128)S(1)} %bitcast.182), channel_id=1, replica_groups=mesh['grp'=2,'sp'=4,'tp'=4] {'tp'}, use_global_device_ids=true, to_apply=%region_3.0 | all-reduce | flops 256 | bytes 2048 | tf_op jit(solution)/shard_map/psum | solution.py:19
  274.1 17.2 %all-gather.23.cloned.1.call-done = bf16[256,2048]{1,0:T(8,128)(2,1)} async-done(((bf16[256,512]{1,0:T(8,128)(2,1)}), bf16[256,2048]{1,0:T(8,128)(2,1)}) %all-gather.23.cloned.1.call-update) | async-done | bytes 1048592 | tf_op jit(solution)/shard_map/all_gather | solution.py:36
  291.2 2.7 fusion.46
  293.9 2.6 fusion.45
  296.6 1.3 collective-permute-start.1
  297.9 0.8 collective-permute-done.1
  298.7 0.0 copy-done.5
  298.7 3.1 fusion.42
  301.8 0.0 all-gather.25.cloned.1.call-update
  301.8 0.0 all-gather.27.cloned.1.call-start
  301.9 30.3 %all-gather.25.cloned.1.call-done = bf16[256,2048]{1,0:T(8,128)(2,1)} async-done(((bf16[256,512]{1,0:T(8,128)(2,1)}), bf16[256,2048]{1,0:T(8,128)(2,1)}) %all-gather.25.cloned.1.call-update) | async-done | bytes 1048592 | tf_op jit(solution)/shard_map/all_gather | solution.py:57
  332.2 3.3 multiply_reduce_fusion.1
  335.5 0.0 all-gather.27.cloned.1.call-update
  335.5 0.0 all-gather.29.cloned.1.call-start
  335.6 10.3 %psum.30 = f32[256,1]{0,1:T(1,128)S(1)} all-reduce(f32[256,1]{0,1:T(1,128)S(1)} %bitcast.181), channel_id=1, replica_groups=mesh['grp'=2,'sp'=4,'tp'=4] {'tp'}, use_global_device_ids=true, to_apply=%region_5.0 | all-reduce | flops 256 | bytes 2048 | tf_op jit(solution)/shard_map/psum | solution.py:19
  345.9 17.2 %all-gather.27.cloned.1.call-done = bf16[256,2048]{1,0:T(8,128)(2,1)} async-done(((bf16[256,512]{1,0:T(8,128)(2,1)}), bf16[256,2048]{1,0:T(8,128)(2,1)}) %all-gather.27.cloned.1.call-update) | async-done | bytes 1048592 | tf_op jit(solution)/shard_map/all_gather | solution.py:36
  363.0 2.7 fusion.53
  365.7 2.6 fusion.52
  368.4 0.0 copy-start.2
  368.4 1.3 collective-permute-start.2
  369.7 0.8 collective-permute-done.2
  370.5 0.0 copy-done.4
  370.5 3.1 fusion.49
  373.6 0.0 all-gather.29.cloned.1.call-update
  373.6 30.3 %all-gather.29.cloned.1.call-done = bf16[256,2048]{1,0:T(8,128)(2,1)} async-done(((bf16[256,512]{1,0:T(8,128)(2,1)}), bf16[256,2048]{1,0:T(8,128)(2,1)}) %all-gather.29.cloned.1.call-update) | async-done | bytes 1048592 | tf_op jit(solution)/shard_map/all_gather | solution.py:57
  404.0 2.7 multiply_reduce_fusion
  406.7 10.2 %psum.31 = f32[256,1]{0,1:T(1,128)S(1)} all-reduce(f32[256,1]{0,1:T(1,128)S(1)} %bitcast.183), channel_id=1, replica_groups=mesh['grp'=2,'sp'=4,'tp'=4] {'tp'}, use_global_device_ids=true, to_apply=%region_7.0 | all-reduce | flops 256 | bytes 2048 | tf_op jit(solution)/shard_map/psum | solution.py:19
  416.8 0.0 copy-done.2
  416.8 0.8 multiply_convert_fusion
  (11 shorter events, 0.1 us)
Async XLA Ops:
  6.5 33.5 %all-gather.11.cloned.1.call-start = ((), (), s32[]{:S(2)}) async-start(), calls=%async_computation | async-start | bytes 1310720 | tf_op jit(solution)/shard_map/all_gather | solution.py:36
  9.1 78.2 %all-gather.17.cloned.1.call-start = ((), (), s32[]{:S(2)}) async-start(), calls=%async_computation.3 | async-start | bytes 7864320 | tf_op jit(solution)/shard_map/all_gather | solution.py:30
  9.9 125.4 %all-gather.15.cloned.1.call-start = ((), (), s32[]{:S(2)}) async-start(), calls=%async_computation.2 | async-start | bytes 7864320 | tf_op jit(solution)/shard_map/all_gather | solution.py:29
  10.6 129.5 %copy-start.1 = (f32[3,3,512]{2,1,0:T(4,128)S(1)}, f32[3,3,512]{2,1,0:T(4,128)}, u32[]{:S(2)}) copy-start(f32[3,3,512]{2,1,0:T(4,128)} %param.13) | copy-start | bytes 55300
  10.6 172.5 %all-gather.13.cloned.1.call-start = ((), (), s32[]{:S(2)}) async-start(), calls=%async_computation.1 | async-start | bytes 7864320 | tf_op jit(solution)/shard_map/all_gather | solution.py:28
  11.2 219.7 %all-gather.21.cloned.1.call-start = ((), (), s32[]{:S(2)}) async-start(), calls=%async_computation.5 | async-start | bytes 7864320 | tf_op jit(solution)/shard_map/all_gather | solution.py:31
  11.8 248.6 %all-gather.19.cloned.1.call-start = ((), (), s32[]{:S(2)}) async-start(), calls=%async_computation.4 | async-start | bytes 1310720 | tf_op jit(solution)/shard_map/all_gather | solution.py:57
  40.0 143.1 %copy-start.3 = (bf16[256,2048]{1,0:T(8,128)(2,1)S(1)}, bf16[256,2048]{1,0:T(8,128)(2,1)}, u32[]{:S(2)}) copy-start(bf16[256,2048]{1,0:T(8,128)(2,1)} %all-gather.11.cloned.1.call-done) | copy-start | bytes 3145732
  90.0 170.4 %copy-start = (bf16[256,512]{1,0:T(8,128)(2,1)S(1)}, bf16[256,512]{1,0:T(8,128)(2,1)}, u32[]{:S(2)}) copy-start(bf16[256,512]{1,0:T(8,128)(2,1)} %param.8) | copy-start | bytes 786436
  137.9 45.2 %collective-permute-start = (bf16[2,512]{1,0:T(2,128)(2,1)S(1)}, bf16[2,512]{1,0:T(2,128)(2,1)S(1)}, u32[]{:S(2)}, u32[]{:S(2)}) collective-permute-start(bf16[2,512]{1,0:T(2,128)(2,1)S(1)} %slice.135), channel_id=1, source_target_pairs={{0,4},{4,8},{8,12},{1,5},{5,9},{9,13},{2,6},{6,10},{10,14},{3,7},{... | collective-permute-start | bytes 6152 | tf_op jit(solution)/shard_map/ppermute | solution.py:15
  186.2 105.0 %all-gather.23.cloned.1.call-start = ((), (), s32[]{:S(2)}) async-start(), calls=%async_computation.6 | async-start | bytes 1310720 | tf_op jit(solution)/shard_map/all_gather | solution.py:36
  263.7 68.4 %all-gather.25.cloned.1.call-start = ((), (), s32[]{:S(2)}) async-start(), calls=%async_computation.7 | async-start | bytes 1310720 | tf_op jit(solution)/shard_map/all_gather | solution.py:57
  291.2 7.5 %copy-start.5 = (bf16[256,2048]{1,0:T(8,128)(2,1)S(1)}, bf16[256,2048]{1,0:T(8,128)(2,1)}, u32[]{:S(2)}) copy-start(bf16[256,2048]{1,0:T(8,128)(2,1)} %all-gather.23.cloned.1.call-done) | copy-start | bytes 3145732
  296.6 2.1 collective-permute-start.1
  301.8 61.2 %all-gather.27.cloned.1.call-start = ((), (), s32[]{:S(2)}) async-start(), calls=%async_computation.8 | async-start | bytes 1310720 | tf_op jit(solution)/shard_map/all_gather | solution.py:36
  335.5 68.4 %all-gather.29.cloned.1.call-start = ((), (), s32[]{:S(2)}) async-start(), calls=%async_computation.9 | async-start | bytes 1310720 | tf_op jit(solution)/shard_map/all_gather | solution.py:57
  363.0 7.5 %copy-start.4 = (bf16[256,2048]{1,0:T(8,128)(2,1)S(1)}, bf16[256,2048]{1,0:T(8,128)(2,1)}, u32[]{:S(2)}) copy-start(bf16[256,2048]{1,0:T(8,128)(2,1)} %all-gather.27.cloned.1.call-done) | copy-start | bytes 3145732
  368.4 48.5 %copy-start.2 = (f32[512]{0:T(512)S(1)}, f32[512]{0:T(512)}, u32[]{:S(2)}) copy-start(f32[512]{0:T(512)} %param.15) | copy-start | bytes 6148
  368.4 2.1 collective-permute-start.2
Sparse Core Ops, SparseCore 0:
  9.2 30.7 all-gather.10
  41.6 45.7 all-gather.16
  88.9 46.3 all-gather.14
  136.7 46.3 all-gather.12
  184.5 46.3 all-gather.20
  232.3 27.9 all-gather.18
  263.8 27.3 all-gather.22
  302.0 30.1 all-gather.24
  335.6 27.3 all-gather.26
  373.8 30.1 all-gather.28
where the time goes:
time: 425 us
  waiting for transfers between devices  323 us (76%)
  blocking collectives  44.2 us (10%)
  matrix products  34.6 us (8%)
  between operations  13.7 us (3%)
  starting transfers between devices  5.1 us (1%)
    all_gather x3, waiting for transfers between devices, shards(): spread = lax.all_gather(gated, 'tp', axis=1, tiled=True)  90 us
    all_gather x3, waiting for transfers between devices, shards(): gathered = lax.all_gather(normed, 'tp', axis=1, tiled=True)  49.1 us
    all_gather x1, waiting for transfers between devices, shards(): lax.all_gather(value_proj, 'sp', axis=1, tiled=True)  47.3 us
    all_gather x1, waiting for transfers between devices, shards(): lax.all_gather(in_gate, 'sp', axis=1, tiled=True)  45.3 us
    all_gather x1, waiting for transfers between devices, shards(): lax.all_gather(mix_proj, 'sp', axis=1, tiled=True)  44.6 us
    psum x4, blocking collectives, row_scale(): squares = lax.psum(jnp.sum(stream * stream, axis=1, keepdims=True), 'tp')  44.2 us
    all_gather x1, waiting for transfers between devices, shards(): lax.all_gather(out_gate, 'sp', axis=1, tiled=True)  43 us
    dot_general x9, matrix products, shards(): jnp.dot(gathered, weight[layer_index], preferred_element_type=jnp.float32)  25.2 us
  transfers between devices with their start and end apart: 13, of which 12 were waited for; matrix products, arithmetic and copies ran while one was open for 2% of the time, Pallas kernels for 0%

commit v1 on v0

--- a/solution.py
+++ b/solution.py
@@ -16,7 +16,7 @@
 
 
 def row_scale(stream):
-    squares = lax.psum(jnp.sum(stream * stream, axis=1, keepdims=True), "tp")
+    squares = jnp.sum(lax.all_gather(jnp.sum(stream * stream, axis=1, keepdims=True), "tp"), axis=0)
     return lax.rsqrt(squares / D + epsilon)
 
 

time: 425 us -> 424 us (level)
    psum x4 -> x0, blocking collectives: 44.2 us -> none  [row_scale(): squares = lax.psum(jnp.sum(stream * stream, axis=1, keepdims=True), 'tp')]
    all_gather x0 -> x4, blocking collectives: none -> 40.8 us  [row_scale(): lax.all_gather(jnp.sum(stream * stream, axis=1, keepdims=True), 'tp')]
where the time goes in v1:
time: 424 us
  waiting for transfers between devices  326 us (77%)
  blocking collectives  40.8 us (10%)
  matrix products  34.6 us (8%)
  between operations  13.7 us (3%)
  starting transfers between devices  5.1 us (1%)
    all_gather x3, waiting for transfers between devices, shards(): spread = lax.all_gather(gated, 'tp', axis=1, tiled=True)  90 us
    all_gather x3, waiting for transfers between devices, shards(): gathered = lax.all_gather(normed, 'tp', axis=1, tiled=True)  51.6 us
    all_gather x1, waiting for transfers between devices, shards(): lax.all_gather(value_proj, 'sp', axis=1, tiled=True)  47.3 us
    all_gather x1, waiting for transfers between devices, shards(): lax.all_gather(in_gate, 'sp', axis=1, tiled=True)  45.3 us
    all_gather x1, waiting for transfers between devices, shards(): lax.all_gather(mix_proj, 'sp', axis=1, tiled=True)  44.6 us
    all_gather x1, waiting for transfers between devices, shards(): lax.all_gather(out_gate, 'sp', axis=1, tiled=True)  43 us
    all_gather x4, blocking collectives, row_scale(): lax.all_gather(jnp.sum(stream * stream, axis=1, keepdims=True), 'tp')  40.8 us
    dot_general x9, matrix products, shards(): jnp.dot(gathered, weight[layer_index], preferred_element_type=jnp.float32)  25.2 us
  transfers between devices with their start and end apart: 13, of which 12 were waited for; matrix products, arithmetic and copies ran while one was open for 2% of the time, Pallas kernels for 0%

profile of v1, /device:TPU:0, one launch (start us, length us, event | category | flops | bytes accessed | tf_op | source)
XLA Modules:
  0.0 423.7 jit_solution(2897231548069800875)
XLA Ops:
  6.5 0.0 all-gather.19.cloned.1.call-start
  6.5 0.8 fusion.60
  7.4 1.7 fusion.55
  9.1 0.0 all-gather.19.cloned.1.call-update
  9.1 0.0 all-gather.25.cloned.1.call-start
  9.2 0.7 all-gather.25.cloned.1.call-update
  9.9 0.0 all-gather.23.cloned.1.call-start
  9.9 0.7 all-gather.23.cloned.1.call-update
  10.6 0.0 copy-start.1
  10.6 0.0 all-gather.21.cloned.1.call-start
  10.7 0.5 all-gather.21.cloned.1.call-update
  11.2 0.0 all-gather.29.cloned.1.call-start
  11.2 0.5 all-gather.29.cloned.1.call-update
  11.8 0.0 all-gather.27.cloned.1.call-start
  11.8 12.7 %all-gather.4 = f32[4,1,256]{2,1,0:T(1,128)S(1)} all-gather(f32[1,1,256]{2,1,0:T(1,128)S(1)} %bitcast.155), channel_id=2, replica_groups=mesh['grp'=2,'sp'=4,'tp'=4] {'tp'}, dimensions={0}, use_global_device_ids=true | all-gather | bytes 5120 | tf_op jit(solution)/shard_map/all_gather | solution.py:19
  24.5 15.4 %all-gather.19.cloned.1.call-done = bf16[256,2048]{1,0:T(8,128)(2,1)} async-done(((bf16[256,512]{1,0:T(8,128)(2,1)}), bf16[256,2048]{1,0:T(8,128)(2,1)}) %all-gather.19.cloned.1.call-update) | async-done | bytes 1048592 | tf_op jit(solution)/shard_map/all_gather | solution.py:36
  40.0 47.3 %all-gather.25.cloned.1.call-done = bf16[3,2048,512]{2,1,0:T(8,128)(2,1)} async-done(((bf16[3,512,512]{2,1,0:T(8,128)(2,1)}), bf16[3,2048,512]{2,1,0:T(8,128)(2,1)}) %all-gather.25.cloned.1.call-update) | async-done | bytes 6291472 | tf_op jit(solution)/shard_map/all_gather | solution.py:30
  87.3 2.6 fusion.39
  89.9 0.0 copy-start
  89.9 45.3 %all-gather.23.cloned.1.call-done = bf16[3,2048,512]{2,1,0:T(8,128)(2,1)} async-done(((bf16[3,512,512]{2,1,0:T(8,128)(2,1)}), bf16[3,2048,512]{2,1,0:T(8,128)(2,1)}) %all-gather.23.cloned.1.call-update) | async-done | bytes 6291472 | tf_op jit(solution)/shard_map/all_gather | solution.py:29
  135.3 2.6 fusion.38
  137.9 2.2 collective-permute-start
  140.1 0.0 copy-done.1
  140.1 43.0 %all-gather.21.cloned.1.call-done = bf16[3,2048,512]{2,1,0:T(8,128)(2,1)} async-done(((bf16[3,512,512]{2,1,0:T(8,128)(2,1)}), bf16[3,2048,512]{2,1,0:T(8,128)(2,1)}) %all-gather.21.cloned.1.call-update) | async-done | bytes 6291472 | tf_op jit(solution)/shard_map/all_gather | solution.py:28
  183.1 0.0 collective-permute-done
  183.1 0.0 copy-done.3
  183.1 3.1 fusion.35
  186.2 0.0 all-gather.27.cloned.1.call-update
  186.2 0.0 all-gather.31.cloned.1.call-start
  186.3 44.6 %all-gather.29.cloned.1.call-done = bf16[3,2048,512]{2,1,0:T(8,128)(2,1)} async-done(((bf16[3,512,512]{2,1,0:T(8,128)(2,1)}), bf16[3,2048,512]{2,1,0:T(8,128)(2,1)}) %all-gather.29.cloned.1.call-update) | async-done | bytes 6291472 | tf_op jit(solution)/shard_map/all_gather | solution.py:31
  230.9 29.4 %all-gather.27.cloned.1.call-done = bf16[256,2048]{1,0:T(8,128)(2,1)} async-done(((bf16[256,512]{1,0:T(8,128)(2,1)}), bf16[256,2048]{1,0:T(8,128)(2,1)}) %all-gather.27.cloned.1.call-update) | async-done | bytes 1048592 | tf_op jit(solution)/shard_map/all_gather | solution.py:57
  260.3 0.0 copy-done
  260.3 3.4 multiply_reduce_fusion.2
  263.7 0.0 all-gather.31.cloned.1.call-update
  263.7 0.0 all-gather.33.cloned.1.call-start
  263.7 9.4 %all-gather.5 = f32[4,1,256]{2,1,0:T(1,128)S(1)} all-gather(f32[1,1,256]{2,1,0:T(1,128)S(1)} %bitcast.168), channel_id=3, replica_groups=mesh['grp'=2,'sp'=4,'tp'=4] {'tp'}, dimensions={0}, use_global_device_ids=true | all-gather | bytes 5120 | tf_op jit(solution)/shard_map/all_gather | solution.py:19
  273.1 18.1 %all-gather.31.cloned.1.call-done = bf16[256,2048]{1,0:T(8,128)(2,1)} async-done(((bf16[256,512]{1,0:T(8,128)(2,1)}), bf16[256,2048]{1,0:T(8,128)(2,1)}) %all-gather.31.cloned.1.call-update) | async-done | bytes 1048592 | tf_op jit(solution)/shard_map/all_gather | solution.py:36
  291.2 2.7 fusion.46
  293.9 2.6 fusion.45
  296.6 1.3 collective-permute-start.1
  297.9 0.8 collective-permute-done.1
  298.7 0.0 copy-done.5
  298.7 3.1 fusion.42
  301.8 0.0 all-gather.33.cloned.1.call-update
  301.8 0.0 all-gather.35.cloned.1.call-start
  301.9 30.3 %all-gather.33.cloned.1.call-done = bf16[256,2048]{1,0:T(8,128)(2,1)} async-done(((bf16[256,512]{1,0:T(8,128)(2,1)}), bf16[256,2048]{1,0:T(8,128)(2,1)}) %all-gather.33.cloned.1.call-update) | async-done | bytes 1048592 | tf_op jit(solution)/shard_map/all_gather | solution.py:57
  332.1 3.3 multiply_reduce_fusion.1
  335.5 0.0 all-gather.35.cloned.1.call-update
  335.5 0.0 all-gather.37.cloned.1.call-start
  335.5 9.4 %all-gather.6 = f32[4,1,256]{2,1,0:T(1,128)S(1)} all-gather(f32[1,1,256]{2,1,0:T(1,128)S(1)} %bitcast.167), channel_id=4, replica_groups=mesh['grp'=2,'sp'=4,'tp'=4] {'tp'}, dimensions={0}, use_global_device_ids=true | all-gather | bytes 5120 | tf_op jit(solution)/shard_map/all_gather | solution.py:19
  344.9 18.1 %all-gather.35.cloned.1.call-done = bf16[256,2048]{1,0:T(8,128)(2,1)} async-done(((bf16[256,512]{1,0:T(8,128)(2,1)}), bf16[256,2048]{1,0:T(8,128)(2,1)}) %all-gather.35.cloned.1.call-update) | async-done | bytes 1048592 | tf_op jit(solution)/shard_map/all_gather | solution.py:36
  363.0 2.7 fusion.53
  365.7 2.6 fusion.52
  368.3 0.0 copy-start.2
  368.4 1.3 collective-permute-start.2
  369.7 0.8 collective-permute-done.2
  370.5 0.0 copy-done.4
  370.5 3.1 fusion.49
  373.6 0.0 all-gather.37.cloned.1.call-update
  373.6 30.3 %all-gather.37.cloned.1.call-done = bf16[256,2048]{1,0:T(8,128)(2,1)} async-done(((bf16[256,512]{1,0:T(8,128)(2,1)}), bf16[256,2048]{1,0:T(8,128)(2,1)}) %all-gather.37.cloned.1.call-update) | async-done | bytes 1048592 | tf_op jit(solution)/shard_map/all_gather | solution.py:57
  403.9 2.7 multiply_reduce_fusion
  406.6 9.4 %all-gather.7 = f32[4,1,256]{2,1,0:T(1,128)S(1)} all-gather(f32[1,1,256]{2,1,0:T(1,128)S(1)} %bitcast.169), channel_id=5, replica_groups=mesh['grp'=2,'sp'=4,'tp'=4] {'tp'}, dimensions={0}, use_global_device_ids=true | all-gather | bytes 5120 | tf_op jit(solution)/shard_map/all_gather | solution.py:19
  416.0 0.0 copy-done.2
  416.0 0.8 multiply_convert_fusion
  (15 shorter events, 0.2 us)
Async XLA Ops:
  6.5 33.4 %all-gather.19.cloned.1.call-start = ((), (), s32[]{:S(2)}) async-start(), calls=%async_computation | async-start | bytes 1310720 | tf_op jit(solution)/shard_map/all_gather | solution.py:36
  9.1 78.2 %all-gather.25.cloned.1.call-start = ((), (), s32[]{:S(2)}) async-start(), calls=%async_computation.3 | async-start | bytes 7864320 | tf_op jit(solution)/shard_map/all_gather | solution.py:30
  9.9 125.4 %all-gather.23.cloned.1.call-start = ((), (), s32[]{:S(2)}) async-start(), calls=%async_computation.2 | async-start | bytes 7864320 | tf_op jit(solution)/shard_map/all_gather | solution.py:29
  10.6 129.5 %copy-start.1 = (f32[3,3,512]{2,1,0:T(4,128)S(1)}, f32[3,3,512]{2,1,0:T(4,128)}, u32[]{:S(2)}) copy-start(f32[3,3,512]{2,1,0:T(4,128)} %param.13) | copy-start | bytes 55300
  10.6 172.5 %all-gather.21.cloned.1.call-start = ((), (), s32[]{:S(2)}) async-start(), calls=%async_computation.1 | async-start | bytes 7864320 | tf_op jit(solution)/shard_map/all_gather | solution.py:28
  11.2 219.7 %all-gather.29.cloned.1.call-start = ((), (), s32[]{:S(2)}) async-start(), calls=%async_computation.5 | async-start | bytes 7864320 | tf_op jit(solution)/shard_map/all_gather | solution.py:31
  11.8 248.5 %all-gather.27.cloned.1.call-start = ((), (), s32[]{:S(2)}) async-start(), calls=%async_computation.4 | async-start | bytes 1310720 | tf_op jit(solution)/shard_map/all_gather | solution.py:57
  40.0 143.1 %copy-start.3 = (bf16[256,2048]{1,0:T(8,128)(2,1)S(1)}, bf16[256,2048]{1,0:T(8,128)(2,1)}, u32[]{:S(2)}) copy-start(bf16[256,2048]{1,0:T(8,128)(2,1)} %all-gather.19.cloned.1.call-done) | copy-start | bytes 3145732
  89.9 170.4 %copy-start = (bf16[256,512]{1,0:T(8,128)(2,1)S(1)}, bf16[256,512]{1,0:T(8,128)(2,1)}, u32[]{:S(2)}) copy-start(bf16[256,512]{1,0:T(8,128)(2,1)} %param.8) | copy-start | bytes 786436
  137.9 45.2 %collective-permute-start = (bf16[2,512]{1,0:T(2,128)(2,1)S(1)}, bf16[2,512]{1,0:T(2,128)(2,1)S(1)}, u32[]{:S(2)}, u32[]{:S(2)}) collective-permute-start(bf16[2,512]{1,0:T(2,128)(2,1)S(1)} %slice.135), channel_id=1, source_target_pairs={{0,4},{4,8},{8,12},{1,5},{5,9},{9,13},{2,6},{6,10},{10,14},{3,7},{... | collective-permute-start | bytes 6152 | tf_op jit(solution)/shard_map/ppermute | solution.py:15
  186.2 105.0 %all-gather.31.cloned.1.call-start = ((), (), s32[]{:S(2)}) async-start(), calls=%async_computation.6 | async-start | bytes 1310720 | tf_op jit(solution)/shard_map/all_gather | solution.py:36
  263.7 68.4 %all-gather.33.cloned.1.call-start = ((), (), s32[]{:S(2)}) async-start(), calls=%async_computation.7 | async-start | bytes 1310720 | tf_op jit(solution)/shard_map/all_gather | solution.py:57
  291.2 7.5 %copy-start.5 = (bf16[256,2048]{1,0:T(8,128)(2,1)S(1)}, bf16[256,2048]{1,0:T(8,128)(2,1)}, u32[]{:S(2)}) copy-start(bf16[256,2048]{1,0:T(8,128)(2,1)} %all-gather.31.cloned.1.call-done) | copy-start | bytes 3145732
  296.6 2.1 collective-permute-start.1
  301.8 61.2 %all-gather.35.cloned.1.call-start = ((), (), s32[]{:S(2)}) async-start(), calls=%async_computation.8 | async-start | bytes 1310720 | tf_op jit(solution)/shard_map/all_gather | solution.py:36
  335.5 68.4 %all-gather.37.cloned.1.call-start = ((), (), s32[]{:S(2)}) async-start(), calls=%async_computation.9 | async-start | bytes 1310720 | tf_op jit(solution)/shard_map/all_gather | solution.py:57
  363.0 7.5 %copy-start.4 = (bf16[256,2048]{1,0:T(8,128)(2,1)S(1)}, bf16[256,2048]{1,0:T(8,128)(2,1)}, u32[]{:S(2)}) copy-start(bf16[256,2048]{1,0:T(8,128)(2,1)} %all-gather.35.cloned.1.call-done) | copy-start | bytes 3145732
  368.3 47.7 %copy-start.2 = (f32[512]{0:T(512)S(1)}, f32[512]{0:T(512)}, u32[]{:S(2)}) copy-start(f32[512]{0:T(512)} %param.15) | copy-start | bytes 6148
  368.4 2.1 collective-permute-start.2
Sparse Core Ops, SparseCore 0:
  9.2 30.7 all-gather.18
  41.5 45.7 all-gather.24
  88.9 46.3 all-gather.22
  136.7 46.3 all-gather.20
  184.5 46.3 all-gather.28
  232.3 27.9 all-gather.26
  263.8 27.3 all-gather.30
  301.9 30.1 all-gather.32
  335.6 27.3 all-gather.34
  373.7 30.1 all-gather.36
